TPU v7x, 32 devices: a whole 2x2x4 slice. The times are simulated.
32 devices in a mesh: sp: 8 (over z, y), tp: 4 (over x, core).
Axes of the slice: x: 2, y: 2, z: 4, core: 2. Of those that a mesh axis runs over, the one named last changes fastest.
Arguments:
- out_grad: bfloat16 [1536, 2048], P('sp'), may hold values from -6 to 6
- routes: int32 [1536, 2], P('sp'), may hold values from 0 to 7, all different within a row; in each aligned block of 192 rows (0 to 191, 192 to 383, ...) at most 96 rows name the same one
- route_weight: float32 [1536, 2], P('sp'), may hold values from 0.3 to 1.5
- expert_rows: bfloat16 [8, 8, 96, 2048], P(None, 'sp'), may hold values from -6 to 6
- gate_weight: bfloat16 [8, 2048, 1024], P('sp', None, 'tp'), may hold values from -0.125 to 0.125
- up_weight: bfloat16 [8, 2048, 1024], P('sp', None, 'tp'), may hold values from -0.125 to 0.125
- down_weight: bfloat16 [8, 1024, 2048], P('sp', 'tp'), may hold values from -0.1875 to 0.1875
- conv_input: bfloat16 [1536, 1024], P('sp', 'tp'), may hold values from -6 to 6
- out_gate: bfloat16 [1536, 1024], P('sp', 'tp'), may hold values from -6 to 6
- in_gate: bfloat16 [1536, 1024], P('sp', 'tp'), may hold values from -6 to 6
- taps: float32 [3, 1024], P(None, 'tp'), may hold values from -3 to 3
- out_weight: bfloat16 [2048, 1024], P(None, 'tp'), may hold values from -0.1875 to 0.1875
Outputs:
- gate_grad: bfloat16 [8, 2048, 1024], P('sp', None, 'tp')
- up_grad: bfloat16 [8, 2048, 1024], P('sp', None, 'tp')
- down_grad: bfloat16 [8, 1024, 2048], P('sp', 'tp')
- mid_grad: bfloat16 [1536, 2048], P('sp', 'tp')
- out_weight_grad: float32 [2048, 1024], P('sp', 'tp')
- input_grad: bfloat16 [1536, 1024], P('sp', 'tp')
- out_gate_grad: bfloat16 [1536, 1024], P('sp', 'tp')
- in_gate_grad: bfloat16 [1536, 1024], P('sp', 'tp')
Inputs may be any that keep to these rules, and one draw needn't show every extreme that they name: `routes`: each token names 2 different experts; within each aligned block of 192 tokens no expert is named by more than 96 tokens, a bound that some block reaches.
All inputs are finite; a program needn't handle non-finite values.
Results may differ from a plain program's by a relative error of at most 0.014.
Values may be sent and summed in bfloat16 or wider, within the bound.
A program may use at most 64 MiB of HBM per device.

v0:
```python
import functools

import jax
import jax.numpy as jnp
from jax import lax
from jax.experimental import pallas as pl
from jax.experimental.pallas import tpu as pltpu
from jax.sharding import PartitionSpec as P

ANY_SPEC = pl.BlockSpec(memory_space=pl.ANY)
VMEM_SPEC = pl.BlockSpec(memory_space=pltpu.VMEM)


def passed_along(shard, axis, by):
    peers = lax.axis_size(axis)
    pairs = [(i, i + by) for i in range(peers) if 0 <= i + by < peers]
    return lax.ppermute(shard, axis, pairs)


def remote(src, dst, send_sem, recv_sem, **target):
    return pltpu.make_async_remote_copy(
        src_ref=src,
        dst_ref=dst,
        send_sem=send_sem,
        recv_sem=recv_sem,
        device_id=target,
        device_id_type=pl.DeviceIdType.MESH,
    )


def greet(sp_peers, tp_peers):
    barrier = pltpu.get_barrier_semaphore()
    for peer in sp_peers:
        pl.semaphore_signal(
            barrier, inc=1, device_id={"sp": peer}, device_id_type=pl.DeviceIdType.MESH
        )
    for peer in tp_peers:
        pl.semaphore_signal(
            barrier, inc=1, device_id={"tp": peer}, device_id_type=pl.DeviceIdType.MESH
        )
    pl.semaphore_wait(barrier, len(sp_peers) + len(tp_peers))


def tp_places(groups):
    member = lax.axis_index("tp")
    sibling = member + 1 - 2 * lax.rem(member, 2)
    others = [lax.rem(member + 2 * d, groups) for d in range(1, groups // 2)]
    return member, sibling, others


def columns(member, share):
    return pl.ds(pl.multiple_of(member * share, share), share)


def spread_kernel(
    n,
    groups,
    send_ref,
    rows_hbm,
    wg_hbm,
    wu_hbm,
    out_ref,
    gate_ref,
    up_ref,
    rows_ref,
    wg_ref,
    wu_ref,
    load_sem,
    own_sem,
    s_a,
    r_a,
    s_f,
    r_f,
    s_g,
    r_g,
):
    me = lax.axis_index("sp")
    member, sibling, others = tp_places(groups)
    share = send_ref.shape[2]
    greet([lax.rem(me + off, n) for off in range(1, n)], [sibling] + others)

    def across(off):
        dest = lax.rem(me + off, n)
        return remote(
            send_ref.at[dest],
            out_ref.at[me, :, columns(member, share)],
            s_a.at[off],
            r_a.at[off],
            sp=dest,
        )

    def block(off, owner):
        return out_ref.at[lax.rem(me + n - off, n), :, columns(owner, share)]

    def hand(off, d):
        target = sibling if d == 0 else others[d - 1]
        return remote(
            block(off, member), block(off, member), s_f.at[d, off], r_f.at[d, off], tp=target
        )

    def relay(off, d):
        piece = block(off, others[d - 1])
        return remote(piece, piece, s_g.at[d - 1, off], r_g.at[d - 1, off], tp=sibling)

    def hand_on(off):
        for d in range(groups // 2):
            hand(off, d).start()

    def relay_on(off):
        for d in range(1, groups // 2):
            hand(off, d).wait_recv()
            relay(off, d).start()

    own = pltpu.make_async_copy(send_ref.at[me], out_ref.at[me, :, columns(member, share)], own_sem)
    own.start()

    def send_out(off, carry):
        across(off).start()
        return carry

    lax.fori_loop(1, n, send_out, 0)
    loads = [
        pltpu.make_async_copy(wg_hbm, wg_ref, load_sem.at[0]),
        pltpu.make_async_copy(wu_hbm, wu_ref, load_sem.at[1]),
        pltpu.make_async_copy(rows_hbm, rows_ref, load_sem.at[2]),
    ]
    for load in loads:
        load.start()
    own.wait()
    hand_on(0)
    tall = rows_ref.shape[0]
    inside = (tall // n) % 16 == 0
    pieces = n if inside else 4
    size = tall // pieces

    def project(piece):
        at = pl.ds(pl.multiple_of(piece * size, size), size)
        rows = rows_ref[at, :]
        gate_ref[at, :] = jnp.dot(rows, wg_ref[...], preferred_element_type=jnp.float32)
        up_ref[at, :] = jnp.dot(rows, wu_ref[...], preferred_element_type=jnp.float32)

    def project_step(piece, carry):
        project(piece)
        return carry

    for load in loads:
        load.wait()
    if inside:
        project(n - 1)
    else:
        lax.fori_loop(0, pieces, project_step, 0)

    def step(off, carry):
        across(off).wait_recv()
        hand_on(off)
        relay_on(off - 1)
        if inside:
            project(off - 1)
        return carry

    lax.fori_loop(1, n, step, 0)
    relay_on(n - 1)

    def finish(off, carry):
        hand(off, 0).wait_recv()
        for d in range(groups // 2):
            hand(off, d).wait_send()
        for d in range(1, groups // 2):
            relay(off, d).wait()
        return carry

    lax.fori_loop(0, n, finish, 0)

    def drain(off, carry):
        across(off).wait_send()
        return carry

    lax.fori_loop(1, n, drain, 0)


def spread(blocks, rows, gate_weight, up_weight, groups):
    n, depth, share = blocks.shape
    hidden = jax.ShapeDtypeStruct((rows.shape[0], gate_weight.shape[1]), jnp.float32)
    dma = pltpu.SemaphoreType.DMA
    return pl.pallas_call(
        functools.partial(spread_kernel, n, groups),
        out_shape=(
            jax.ShapeDtypeStruct((n, depth, share * groups), blocks.dtype),
            hidden,
            hidden,
        ),
        in_specs=[VMEM_SPEC, ANY_SPEC, ANY_SPEC, ANY_SPEC],
        out_specs=(VMEM_SPEC, VMEM_SPEC, VMEM_SPEC),
        scratch_shapes=[
            pltpu.VMEM(rows.shape, rows.dtype),
            pltpu.VMEM(gate_weight.shape, gate_weight.dtype),
            pltpu.VMEM(up_weight.shape, up_weight.dtype),
            dma((3,)),
            dma(()),
            dma((n,)),
            dma((n,)),
            dma((groups // 2, n)),
            dma((groups // 2, n)),
            dma((groups // 2 - 1, n)),
            dma((groups // 2 - 1, n)),
        ],
        compiler_params=pltpu.CompilerParams(collective_id=0, has_side_effects=True),
    )(blocks, rows, gate_weight, up_weight)


def collect_kernel(
    n,
    groups,
    part_ref,
    rows_hbm,
    grads_hbm,
    act_hbm,
    gate_hbm,
    up_hbm,
    out_ref,
    gate_out,
    up_out,
    down_out,
    near,
    pair,
    far,
    final,
    rows_ref,
    grads_ref,
    act_ref,
    gate_ref,
    up_ref,
    load_sem,
    s_n,
    r_n,
    s_f,
    r_f,
    s_a,
    r_a,
):
    me = lax.axis_index("sp")
    member, sibling, others = tp_places(groups)
    half = groups // 2
    share = out_ref.shape[2]
    seat, row = lax.rem(member, 2), lax.div(member, 2)
    greet([lax.rem(me + off, n) for off in range(1, n)], [sibling] + others)

    def home(off):
        return lax.rem(me + off, n)

    def to_sibling(off, h):
        return remote(
            part_ref.at[home(off), :, columns(2 * h + 1 - seat, share)],
            near.at[home(off), h],
            s_n.at[h, off],
            r_n.at[h, off],
            tp=sibling,
        )

    def to_other(off, d):
        h = lax.rem(row + d, half)
        return remote(
            pair.at[home(off), h],
            far.at[d - 1, home(off)],
            s_f.at[d - 1, off],
            r_f.at[d - 1, off],
            tp=others[d - 1],
        )

    def to_home(off):
        return remote(
            final.at[home(off)], out_ref.at[me], s_a.at[off], r_a.at[off], sp=home(off)
        )

    def open_step(i, carry):
        off = lax.rem(i + 1, n)
        for h in range(half):
            to_sibling(off, h).start()
        return carry

    lax.fori_loop(0, n, open_step, 0)
    sources = (act_hbm, gate_hbm, up_hbm, rows_hbm, grads_hbm)
    held = (act_ref, gate_ref, up_ref, rows_ref, grads_ref)
    loads = [pltpu.make_async_copy(a, b, load_sem.at[i]) for i, (a, b) in enumerate(zip(sources, held))]
    for load in loads:
        load.start()
    width = rows_ref.shape[1]
    inside = width % (128 * n) == 0
    pieces = n if inside else 8
    size = width // pieces

    def across_rows(a, b):
        total = lax.dot_general(a, b, (((0,), (0,)), ((), ())), preferred_element_type=jnp.float32)
        return total.astype(jnp.bfloat16)

    def weigh(piece):
        at = columns(piece, size)
        rows = rows_ref[:, at]
        gate_out[at, :] = across_rows(rows, gate_ref[...])
        up_out[at, :] = across_rows(rows, up_ref[...])
        down_out[:, at] = across_rows(act_ref[...], grads_ref[:, at])

    def weigh_step(piece, carry):
        weigh(piece)
        return carry

    def pair_step(i, carry):
        off = lax.rem(i + 1, n)
        for h in range(half):
            to_sibling(off, h).wait_recv()
            mine = part_ref[home(off), :, columns(2 * h + seat, share)].astype(jnp.float32)
            total = mine + near[home(off), h].astype(jnp.float32)
            pair[home(off), h] = total.astype(jnp.bfloat16)
        for d in range(1, half):
            to_other(off, d).start()
        return carry

    lax.fori_loop(0, n, pair_step, 0)

    for load in loads:
        load.wait()
    if inside:
        weigh(n - 1)
    else:
        lax.fori_loop(0, pieces, weigh_step, 0)

    def summed(off):
        total = pair[home(off), row].astype(jnp.float32)
        for d in range(1, half):
            to_other(off, d).wait_recv()
            total = total + far[d - 1, home(off)].astype(jnp.float32)
        return total.astype(jnp.bfloat16)

    def home_step(off, carry):
        final[home(off)] = summed(off)
        to_home(off).start()
        if inside:
            weigh(off - 1)
        return carry

    lax.fori_loop(1, n, home_step, 0)
    out_ref[me] = summed(0)

    def drain(off, carry):
        for h in range(half):
            to_sibling(off, h).wait_send()
        for d in range(1, half):
            to_other(off, d).wait_send()
        return carry

    lax.fori_loop(0, n, drain, 0)

    def arrive(off, carry):
        to_home(off).wait()
        return carry

    lax.fori_loop(1, n, arrive, 0)


def collect(parts, rows, grads, act, gate_part, up_part, groups):
    n, depth, width = parts.shape
    ff = act.shape[1]
    share, half = width // groups, groups // 2
    dma = pltpu.SemaphoreType.DMA
    return pl.pallas_call(
        functools.partial(collect_kernel, n, groups),
        out_shape=(
            jax.ShapeDtypeStruct((n, depth, share), parts.dtype),
            jax.ShapeDtypeStruct((width, ff), parts.dtype),
            jax.ShapeDtypeStruct((width, ff), parts.dtype),
            jax.ShapeDtypeStruct((ff, width), parts.dtype),
        ),
        in_specs=[VMEM_SPEC] + [ANY_SPEC] * 5,
        out_specs=(VMEM_SPEC,) * 4,
        scratch_shapes=[
            pltpu.VMEM((n, half, depth, share), parts.dtype),
            pltpu.VMEM((n, half, depth, share), parts.dtype),
            pltpu.VMEM((half - 1, n, depth, share), parts.dtype),
            pltpu.VMEM((n, depth, share), parts.dtype),
            pltpu.VMEM(rows.shape, rows.dtype),
            pltpu.VMEM(grads.shape, grads.dtype),
            pltpu.VMEM(act.shape, act.dtype),
            pltpu.VMEM(act.shape, act.dtype),
            pltpu.VMEM(act.shape, act.dtype),
            dma((5,)),
            dma((half, n)),
            dma((half, n)),
            dma((half - 1, n)),
            dma((half - 1, n)),
            dma((n,)),
            dma((n,)),
        ],
        compiler_params=pltpu.CompilerParams(collective_id=1, has_side_effects=True),
    )(parts, rows, grads, act, gate_part, up_part)


def widen_kernel(groups, chunks, own_ref, out_ref, own_sem, s_f, r_f, s_g, r_g):
    member, sibling, others = tp_places(groups)
    rows, share = own_ref.shape
    size = rows // chunks
    greet([], [sibling] + others)

    def place(c, owner):
        return out_ref.at[pl.ds(c * size, size), columns(owner, share)]

    def hand(c, d):
        target = sibling if d == 0 else others[d - 1]
        return remote(
            own_ref.at[pl.ds(c * size, size)],
            place(c, member),
            s_f.at[d, c],
            r_f.at[d, c],
            tp=target,
        )

    def relay(c, d):
        piece = place(c, others[d - 1])
        return remote(piece, piece, s_g.at[d - 1, c], r_g.at[d - 1, c], tp=sibling)

    for c in range(chunks):
        for d in range(1, groups // 2):
            hand(c, d).start()
    for c in range(chunks):
        hand(c, 0).start()
    own = pltpu.make_async_copy(own_ref, out_ref.at[:, columns(member, share)], own_sem)
    own.start()
    for c in range(chunks):
        for d in range(1, groups // 2):
            hand(c, d).wait_recv()
            relay(c, d).start()
    own.wait()
    for c in range(chunks):
        hand(c, 0).wait_recv()
        for d in range(groups // 2):
            hand(c, d).wait_send()
        for d in range(1, groups // 2):
            relay(c, d).wait()


def widen(own, groups):
    rows, share = own.shape
    chunks = 4 if rows % 64 == 0 else 1
    dma = pltpu.SemaphoreType.DMA
    return pl.pallas_call(
        functools.partial(widen_kernel, groups, chunks),
        out_shape=jax.ShapeDtypeStruct((rows, share * groups), own.dtype),
        in_specs=[VMEM_SPEC],
        out_specs=VMEM_SPEC,
        scratch_shapes=[
            dma(()),
            dma((groups // 2, chunks)),
            dma((groups // 2, chunks)),
            dma((groups // 2 - 1, chunks)),
            dma((groups // 2 - 1, chunks)),
        ],
        compiler_params=pltpu.CompilerParams(collective_id=2, has_side_effects=True),
    )(own)


def fold_kernel(n, part_ref, out_ref, near, pair, far, s_n, r_n, s_f, r_f):
    me = lax.axis_index("sp")
    seat, row = lax.rem(me, 2), lax.div(me, 2)
    partner = me + 1 - 2 * seat
    half = n // 2
    greet([partner] + [lax.rem(me + 2 * d, n) for d in range(1, half)], [])

    def spot(d):
        return lax.rem(row + d, half)

    def to_partner(d):
        return remote(
            part_ref.at[2 * spot(d) + 1 - seat], near.at[d], s_n.at[d], r_n.at[d], sp=partner
        )

    def to_owner(d):
        return remote(
            pair.at[d], far.at[d], s_f.at[d], r_f.at[d], sp=lax.rem(me + 2 * d, n)
        )

    def open_step(i, carry):
        to_partner(lax.rem(i + 1, half)).start()
        return carry

    lax.fori_loop(0, half, open_step, 0)

    def paired(d):
        to_partner(d).wait_recv()
        mine = part_ref[2 * spot(d) + seat].astype(jnp.float32)
        return mine + near[d].astype(jnp.float32)

    def pair_step(d, carry):
        pair[d] = paired(d).astype(jnp.bfloat16)
        to_owner(d).start()
        return carry

    lax.fori_loop(1, half, pair_step, 0)
    out_ref[...] = paired(0)

    def add_step(d, carry):
        to_owner(d).wait_recv()
        out_ref[...] += far[d].astype(jnp.float32)
        return carry

    lax.fori_loop(1, half, add_step, 0)

    def drain(d, carry):
        to_partner(d).wait_send()
        return carry

    lax.fori_loop(0, half, drain, 0)

    def drain_owner(d, carry):
        to_owner(d).wait_send()
        return carry

    lax.fori_loop(1, half, drain_owner, 0)


def fold(parts):
    n, rows, cols = parts.shape
    half = n // 2
    dma = pltpu.SemaphoreType.DMA
    return pl.pallas_call(
        functools.partial(fold_kernel, n),
        out_shape=jax.ShapeDtypeStruct((rows, cols), jnp.float32),
        in_specs=[VMEM_SPEC],
        out_specs=VMEM_SPEC,
        scratch_shapes=[
            pltpu.VMEM((half, rows, cols), parts.dtype),
            pltpu.VMEM((half, rows, cols), parts.dtype),
            pltpu.VMEM((half, rows, cols), parts.dtype),
            dma((half,)),
            dma((half,)),
            dma((half,)),
            dma((half,)),
        ],
        compiler_params=pltpu.CompilerParams(collective_id=3, has_side_effects=True),
    )(parts)


def on_device(
    out_grad,
    routes,
    route_weight,
    expert_rows,
    gate_weight,
    up_weight,
    down_weight,
    conv_input,
    out_gate,
    in_gate,
    taps,
    out_weight,
):
    groups = lax.axis_size("tp")
    member = lax.axis_index("tp")
    sources = lax.axis_size("sp")
    tok_rows, width = out_grad.shape
    top = routes.shape[1]
    local = gate_weight.shape[0]
    assert local == 1
    experts = local * sources
    slots = expert_rows.shape[2]
    share = width // groups
    own_cols = lax.dynamic_slice_in_dim(out_grad, member * share, share, 1)
    names = jnp.arange(experts, dtype=jnp.int32)
    named = routes[:, :, None] == names[None, None, :]
    chosen = jnp.any(named, axis=1)
    weight = jnp.sum(jnp.where(named, route_weight[:, :, None], 0.0), axis=1)
    order = jnp.arange(tok_rows, dtype=jnp.int32)
    earlier = (order[:, None] > order[None, :]).astype(jnp.bfloat16)
    place = jnp.dot(
        earlier, chosen.astype(jnp.bfloat16), preferred_element_type=jnp.float32
    ).astype(jnp.int32)
    place = jnp.where(chosen, place, -1).T
    filled = place[:, None, :] == jnp.arange(slots, dtype=jnp.int32)[None, :, None]
    slot_weight = jnp.sum(jnp.where(filled, weight.T[:, None, :], 0.0), axis=2)
    picker = filled.astype(jnp.bfloat16).reshape(experts * slots, tok_rows)
    outgoing = jnp.dot(picker, own_cols, preferred_element_type=jnp.float32)
    outgoing = (slot_weight.reshape(-1, 1) * outgoing).astype(jnp.bfloat16)
    outgoing = outgoing.reshape(sources, local * slots, share)
    rows = expert_rows.reshape(-1, width)
    wide_gate, wide_up, tall_down = gate_weight[0], up_weight[0], down_weight[0]
    grads, gate, up = spread(outgoing, rows, wide_gate, wide_up, groups)
    grads = grads.reshape(-1, width)
    sig = jax.nn.sigmoid(gate)
    act = (gate * sig * up).astype(jnp.bfloat16)
    act_grad = lax.dot_general(
        grads, tall_down, (((1,), (1,)), ((), ())), preferred_element_type=jnp.float32
    )
    up_part = (act_grad * gate * sig).astype(jnp.bfloat16)
    gate_part = (act_grad * up * sig * (1.0 + gate * (1.0 - sig))).astype(jnp.bfloat16)
    row_part = lax.dot_general(
        gate_part, wide_gate, (((1,), (1,)), ((), ())), preferred_element_type=jnp.float32
    )
    row_part = row_part + lax.dot_general(
        up_part, wide_up, (((1,), (1,)), ((), ())), preferred_element_type=jnp.float32
    )
    row_part = row_part.astype(jnp.bfloat16).reshape(sources, slots, width)
    returned, gate_grad, up_grad, down_grad = collect(
        row_part, rows, grads, act, gate_part, up_part, groups
    )
    returned = returned.reshape(experts * slots, share)
    gate_grad, up_grad, down_grad = gate_grad[None], up_grad[None], down_grad[None]
    picked = lax.dot_general(
        picker, returned, (((0,), (0,)), ((), ())), preferred_element_type=jnp.float32
    )
    mid_grad = (own_cols.astype(jnp.float32) + picked).astype(jnp.bfloat16)
    mid_whole = widen(mid_grad, groups)
    reach = taps.shape[0] - 1
    rims = jnp.stack([in_gate[tok_rows - reach :], conv_input[tok_rows - reach :]])
    prior = passed_along(rims, "sp", 1)
    mixed = in_gate.astype(jnp.float32) * conv_input.astype(jnp.float32)
    prior_mixed = prior[0].astype(jnp.float32) * prior[1].astype(jnp.float32)
    extended = jnp.concatenate([prior_mixed, mixed], axis=0)
    conv = jnp.zeros_like(mixed)
    for tap in range(reach + 1):
        conv = conv + taps[tap][None, :] * extended[reach - tap : reach - tap + tok_rows]
    gated = (out_gate.astype(jnp.float32) * conv).astype(jnp.bfloat16)
    partial_grad = lax.dot_general(
        mid_whole, gated, (((0,), (0,)), ((), ())), preferred_element_type=jnp.float32
    ).astype(jnp.bfloat16)
    out_weight_grad = fold(partial_grad.reshape(sources, width // sources, gated.shape[1]))
    gated_grad = jnp.dot(mid_whole, out_weight, preferred_element_type=jnp.float32)
    out_gate_grad = (gated_grad * conv).astype(jnp.bfloat16)
    conv_grad = gated_grad * out_gate.astype(jnp.float32)
    later = passed_along(conv_grad[:reach], "sp", -1)
    following = jnp.concatenate([conv_grad, later], axis=0)
    mixed_grad = jnp.zeros_like(conv_grad)
    for tap in range(reach + 1):
        mixed_grad = mixed_grad + taps[tap][None, :] * following[tap : tap + tok_rows]
    input_grad = (mixed_grad * in_gate.astype(jnp.float32)).astype(jnp.bfloat16)
    in_gate_grad = (mixed_grad * conv_input.astype(jnp.float32)).astype(jnp.bfloat16)
    return (
        gate_grad,
        up_grad,
        down_grad,
        mid_grad,
        out_weight_grad,
        input_grad,
        out_gate_grad,
        in_gate_grad,
    )


def solution(mesh):
    in_specs = (
        P("sp", None),
        P("sp", None),
        P("sp", None),
        P(None, "sp", None, None),
        P("sp", None, "tp"),
        P("sp", None, "tp"),
        P("sp", "tp", None),
        P("sp", "tp"),
        P("sp", "tp"),
        P("sp", "tp"),
        P(None, "tp"),
        P(None, "tp"),
    )
    out_specs = (
        P("sp", None, "tp"),
        P("sp", None, "tp"),
        P("sp", "tp", None),
        P("sp", "tp"),
        P("sp", "tp"),
        P("sp", "tp"),
        P("sp", "tp"),
        P("sp", "tp"),
    )
    return jax.shard_map(
        on_device, mesh=mesh, in_specs=in_specs, out_specs=out_specs, check_vma=False
    )
```

profile of v0, /device:TPU:1, one launch (start us, length us, event | category | flops | bytes accessed | tf_op | source)
XLA Modules:
  0.0 137.8 jit_solution(14378824583245096890)
XLA Ops:
  0.6 0.8 slice_bitcast_fusion
  1.5 4.0 %collective-permute-start = (bf16[2,2,256]{2,1,0:T(2,128)(2,1)S(1)}, bf16[2,2,256]{2,1,0:T(2,128)(2,1)S(1)}, u32[]{:S(2)}, u32[]{:S(2)}) collective-permute-start(bf16[2,2,256]{2,1,0:T(2,128)(2,1)S(1)} %pad_maximum_fusion.2), channel_id=1, source_target_pairs={{0,4},{4,8},{8,12},{12,16},{16,20},{20,24},{24,28},{1,5},{5,9},{9,... | collective-permute-start | bytes 6152 | tf_op jit(solution)/shard_map/ppermute | solution.py:17
  5.4 1.0 convert_multiply_fusion.1
  6.4 0.7 fusion.23
  7.1 0.1 fusion.2
  7.2 0.1 copy.26
  7.4 0.3 iota_compare_fusion
  7.7 0.3 eq.40
  7.9 0.3 eq.43
  8.2 0.7 select_reduce_fusion.1
  8.9 0.1 copy.27
  9.0 0.6 select_reduce_fusion
  9.8 2.2 %multiply_convert_fusion = bf16[768,512]{1,0:T(8,128)(2,1)} fusion(f32[768]{0:T(1024)S(1)} %mul.109, s32[768,192]{0,1:T(8,128)S(1)} %eq.43, s32[768]{0:T(1024)S(1)} %eq.45, bf16[192,2048]{1,0:T(8,128)(2,1)} %param.12, s32[]{:T(128)S(6)} %select_n.19), kind=kOutput, calls=%fused_computation.2 | convolution fusion | flops 151928832 | bytes 1579012 | tf_op jit(solution)/shard_map/dot_general | solution.py:579
  12.0 35.8 %shard_map.179 = (bf16[8,96,2048]{2,1,0:T(8,128)(2,1)}, f32[768,256]{1,0:T(8,128)}, f32[768,256]{1,0:T(8,128)}) custom-call(bf16[8,96,512]{2,1,0:T(8,128)(2,1)} %bitcast.53, bf16[768,2048]{1,0:T(8,128)(2,1)} %bitcast.47, bf16[2048,256]{1,0:T(8,128)(2,1)} %bitcast.51, bf16[2048,256]{1,0:T(8,128)(2,1)} %bitcast.52), custom_call_target="tpu_custom_call" | custom-call | tf_op jit(solution)/shard_map/pallas_call | solution.py:185
  47.9 4.4 %multiply_convert_fusion.1 = (bf16[768,256]{1,0:T(8,128)(2,1)}, bf16[768,256]{1,0:T(8,128)(2,1)S(1)}, bf16[768,256]{1,0:T(8,128)(2,1)S(1)}) fusion(f32[768,256]{1,0:T(8,128)} %get-tuple-element.16, f32[768,256]{1,0:T(8,128)} %get-tuple-element.17, bf16[768,2048]{1,0:T(8,128)(2,1)} %bitcast.54, bf16[1,256,2048]{2,1,0:T(8,128)(2,1)S(1)} %copy-done), kind=kOutput, calls=%fused_computation.10 | convolution fusion | flops 808452096 | bytes 6946816 | tf_op jit(solution)/shard_map/dot_general | solution.py:588
  52.3 1.0 fusion.26
  53.3 0.5 copy-done.2
  53.8 2.7 %add_convert_fusion = bf16[768,2048]{1,0:T(8,128)(2,1)} fusion(f32[768,2048]{1,0:T(8,128)S(1)} %fusion.26, bf16[768,256]{1,0:T(8,128)(2,1)S(1)} %get-tuple-element.28.up_hbm, bf16[1,2048,256]{2,1,0:T(8,128)(2,1)S(1)} %copy-done.2), kind=kOutput, calls=%fused_computation | convolution fusion | flops 808452096 | bytes 10878976 | tf_op jit(solution)/shard_map/dot_general | solution.py:596
  56.4 33.3 %shard_map.180 = (bf16[8,96,512]{2,1,0:T(8,128)(2,1)}, bf16[2048,256]{1,0:T(8,128)(2,1)}, bf16[2048,256]{1,0:T(8,128)(2,1)}, bf16[256,2048]{1,0:T(8,128)(2,1)}) custom-call(bf16[8,96,2048]{2,1,0:T(8,128)(2,1)} %bitcast.49, bf16[768,2048]{1,0:T(8,128)(2,1)} %bitcast.48, bf16[768,2048]{1,0:T(8,128)(2,1)} %bitcast.55, ...), custom_call_target="tpu_custom_call" | custom-call | tf_op jit(solution)/shard_map/pallas_call | solution.py:365
  89.7 2.2 %fusion.1.own_ref = bf16[192,512]{1,0:T(8,128)(2,1)} fusion(bf16[8,96,512]{2,1,0:T(8,128)(2,1)} %get-tuple-element.21, pred[8,96,192]{1,0,2:T(8,128)(4,1)S(1)} %iota_compare_fusion, bf16[192,2048]{1,0:T(8,128)(2,1)} %param.12, s32[]{:T(128)S(6)} %select_n.19), kind=kOutput, calls=%fused_computation.5 | convolution fusion | flops 151289856 | bytes 1327108 | tf_op jit(solution)/shard_map/dot_general | solution.py:605
  91.9 10.5 %shard_map.181 = bf16[192,2048]{1,0:T(8,128)(2,1)} custom-call(bf16[192,512]{1,0:T(8,128)(2,1)} %fusion.1.own_ref), custom_call_target="tpu_custom_call" | custom-call | tf_op jit(solution)/shard_map/pallas_call | solution.py:444
  102.5 2.2 %multiply_convert_fusion.4 = (bf16[192,256]{1,0:T(8,128)(2,1)}, f32[192,256]{1,0:T(8,128)S(1)}, f32[192,256]{1,0:T(8,128)S(1)}) fusion(f32[192,256]{1,0:T(8,128)S(1)} %convert_multiply_fusion.1, f32[2,256]{1,0:T(2,128)S(1)} %multiply_bitcast_fusion, f32[256]{0:T(256)S(1)} %bitcast.62, f32[256]{0:T(256)S(1)} %bitcast.64, f32[256]{0:T(256)S(1)} %bitcast.60, ...), kind=kOutput, calls=%fused_computation.43 | convolution fusion | flops 201867264 | bytes 2626560 | tf_op jit(solution)/shard_map/dot_general | solution.py:624
  104.7 0.6 slice.55
  105.3 1.3 collective-permute-start.1
  106.6 2.7 %convolution_convert_fusion = bf16[2048,256]{1,0:T(8,128)(2,1)} fusion(bf16[192,2048]{1,0:T(8,128)(2,1)} %shard_map.181, f32[192,256]{1,0:T(8,128)S(1)} %get-tuple-element.25, bf16[192,256]{1,0:T(8,128)(2,1)S(1)} %copy-done.11), kind=kOutput, calls=%fused_computation.1 | convolution fusion | flops 201998336 | bytes 2129920 | tf_op jit(solution)/shard_map/dot_general | solution.py:620
  109.3 22.1 %shard_map.182 = f32[256,256]{1,0:T(8,128)} custom-call(bf16[8,256,256]{2,1,0:T(8,128)(2,1)} %bitcast.50), custom_call_target="tpu_custom_call" | custom-call | tf_op jit(solution)/shard_map/pallas_call | solution.py:523
  131.4 0.7 fusion.18
  132.1 0.7 fusion.17
  132.8 2.3 %copy.35 = bf16[1,2048,256]{2,1,0:T(8,128)(2,1)} copy(bf16[1,2048,256]{2,1,0:T(8,128)(2,1)} %bitcast.58) | data formatting | bytes 2097152
  135.1 1.0 copy.36
  136.1 1.0 copy.37
  137.1 0.7 copy.38
  (33 shorter events, 0.2 us)
Async XLA Ops:
  0.6 47.2 %copy-start = (bf16[1,256,2048]{2,1,0:T(8,128)(2,1)S(1)}, bf16[1,256,2048]{2,1,0:T(8,128)(2,1)}, u32[]{:S(2)}) copy-start(bf16[1,256,2048]{2,1,0:T(8,128)(2,1)} %param.18) | copy-start | bytes 3145732
  1.5 101.0 %collective-permute-start = (bf16[2,2,256]{2,1,0:T(2,128)(2,1)S(1)}, bf16[2,2,256]{2,1,0:T(2,128)(2,1)S(1)}, u32[]{:S(2)}, u32[]{:S(2)}) collective-permute-start(bf16[2,2,256]{2,1,0:T(2,128)(2,1)S(1)} %pad_maximum_fusion.2), channel_id=1, source_target_pairs={{0,4},{4,8},{8,12},{12,16},{16,20},{20,24},{24,28},{1,5},{5,9},{9,... | collective-permute-start | bytes 6152 | tf_op jit(solution)/shard_map/ppermute | solution.py:17
  47.8 4.4 %copy-start.1 = (bf16[1,2048,256]{2,1,0:T(8,128)(2,1)S(1)}, bf16[1,2048,256]{2,1,0:T(8,128)(2,1)}, u32[]{:S(2)}) copy-start(bf16[1,2048,256]{2,1,0:T(8,128)(2,1)} %param.16) | copy-start | bytes 3145732
  52.2 1.0 copy-start.3
  52.2 1.0 copy-start.4
  52.2 1.5 %copy-start.2 = (bf16[1,2048,256]{2,1,0:T(8,128)(2,1)S(1)}, bf16[1,2048,256]{2,1,0:T(8,128)(2,1)}, u32[]{:S(2)}) copy-start(bf16[1,2048,256]{2,1,0:T(8,128)(2,1)} %param.17) | copy-start | bytes 3145732
  56.4 35.5 %copy-start.12 = (f32[3,256]{1,0:T(4,128)S(1)}, f32[3,256]{1,0:T(4,128)}, u32[]{:S(2)}) copy-start(f32[3,256]{1,0:T(4,128)} %param.22) | copy-start | bytes 9220
  56.4 46.1 %copy-start.6 = (bf16[2048,256]{1,0:T(8,128)(2,1)S(1)}, bf16[2048,256]{1,0:T(8,128)(2,1)}, u32[]{:S(2)}) copy-start(bf16[2048,256]{1,0:T(8,128)(2,1)} %param.23) | copy-start | bytes 3145732
  56.4 46.1 %copy-start.11 = (bf16[192,256]{1,0:T(8,128)(2,1)S(1)}, bf16[192,256]{1,0:T(8,128)(2,1)}, u32[]{:S(2)}) copy-start(bf16[192,256]{1,0:T(8,128)(2,1)} %param.20) | copy-start | bytes 294916
  102.5 28.9 %copy-start.9 = (bf16[192,256]{1,0:T(8,128)(2,1)S(1)}, bf16[192,256]{1,0:T(8,128)(2,1)}, u32[]{:S(2)}) copy-start(bf16[192,256]{1,0:T(8,128)(2,1)} %param.19) | copy-start | bytes 294916
  102.5 29.6 %copy-start.10 = (bf16[192,256]{1,0:T(8,128)(2,1)S(1)}, bf16[192,256]{1,0:T(8,128)(2,1)}, u32[]{:S(2)}) copy-start(bf16[192,256]{1,0:T(8,128)(2,1)} %param.21) | copy-start | bytes 294916
  105.3 26.1 %collective-permute-start.1 = (f32[2,256]{1,0:T(2,128)}, f32[2,256]{1,0:T(2,128)S(1)}, u32[]{:S(2)}, u32[]{:S(2)}) collective-permute-start(f32[2,256]{1,0:T(2,128)} %slice.55), channel_id=1, source_target_pairs={{4,0},{8,4},{12,8},{16,12},{20,16},{24,20},{28,24},{5,1},{9,5},{13... | collective-permute-start | bytes 6152 | tf_op jit(solution)/shard_map/ppermute | solution.py:17
  106.6 28.5 %copy-start.8 = (bf16[2048,256]{1,0:T(8,128)(2,1)S(1)}, bf16[2048,256]{1,0:T(8,128)(2,1)}, u32[]{:S(2)}) copy-start(bf16[2048,256]{1,0:T(8,128)(2,1)} %get-tuple-element.19) | copy-start | bytes 3145732
  109.3 26.8 %copy-start.7 = (bf16[256,2048]{1,0:T(8,128)(2,1)S(1)}, bf16[256,2048]{1,0:T(8,128)(2,1)}, u32[]{:S(2)}) copy-start(bf16[256,2048]{1,0:T(8,128)(2,1)} %get-tuple-element.20) | copy-start | bytes 3145732
  132.8 4.3 %copy-start.5 = (f32[256,256]{1,0:T(8,128)S(1)}, f32[256,256]{1,0:T(8,128)}, u32[]{:S(2)}) copy-start(f32[256,256]{1,0:T(8,128)} %shard_map.182) | copy-start | bytes 786436
where the time goes:
time: 140 us; the launch traced here: 138 us
  Pallas kernels  102 us (73%)
  matrix products  17.6 us (13%)
  local copies, waits for them, and re-layouts  7.77 us (6%)
  starting transfers between devices  5.24 us (4%)
  other arithmetic  4.61 us (3%)
    pallas_call x1, Pallas kernels, spread(): pl.pallas_call(functools.partial(spread_kernel, n, groups), out_shape=(ja...  35.8 us
    pallas_call x1, Pallas kernels, collect(): pl.pallas_call(functools.partial(collect_kernel, n, groups), out_shape=(j...  33.3 us
    pallas_call x1, Pallas kernels, fold(): pl.pallas_call(functools.partial(fold_kernel, n), out_shape=jax.ShapeDtyp...  22.1 us
    pallas_call x1, Pallas kernels, widen(): pl.pallas_call(functools.partial(widen_kernel, groups, chunks), out_shape...  10.5 us
    unnamed x30, local copies, waits for them, and re-layouts  5.47 us
    ppermute x2, starting transfers between devices, passed_along(): return lax.ppermute(shard, axis, pairs)  5.24 us
    dot_general x1, matrix products, on_device(): lax.dot_general(grads, tall_down, (((1,), (1,)), ((), ())), preferred_ele...  4.38 us
  transfers between devices with their start and end apart: 2, of which 0 were waited for; matrix products, arithmetic and copies ran while one was open for 14% of the time, Pallas kernels for 74%

commit v1 on v0

--- a/solution.py
+++ b/solution.py
@@ -538,7 +538,658 @@
     )(parts)
 
 
+BF16, F32 = jnp.bfloat16, jnp.float32
+
+
+def dot_nn(a, b):
+    return jnp.dot(a, b, preferred_element_type=F32)
+
+
+def dot_nt(a, b):
+    return lax.dot_general(a, b, (((1,), (1,)), ((), ())), preferred_element_type=F32)
+
+
+def dot_tn(a, b):
+    return lax.dot_general(a, b, (((0,), (0,)), ((), ())), preferred_element_type=F32)
+
+
+def fused_kernel(
+    n,
+    groups,
+    out_grad,
+    routes,
+    route_weight,
+    conv_input,
+    out_gate,
+    in_gate,
+    taps,
+    rows_hbm,
+    wg_hbm,
+    wu_hbm,
+    dn_hbm,
+    ow_hbm,
+    gate_out,
+    up_out,
+    down_out,
+    mid_out,
+    weight_out,
+    input_out,
+    out_gate_out,
+    in_gate_out,
+    rows,
+    wgu,
+    dn,
+    ow,
+    hidden,
+    place,
+    weight,
+    picker,
+    send,
+    grads,
+    act,
+    parts,
+    row_part,
+    near,
+    pair,
+    far,
+    final,
+    back,
+    total,
+    wide,
+    rim,
+    mixed,
+    conv,
+    gated,
+    slices,
+    follow,
+    later,
+    load_sem,
+    s_a,
+    r_a,
+    s_x,
+    r_x,
+    s_b,
+    r_b,
+    s_g,
+    r_g,
+    s_n,
+    r_n,
+    s_f,
+    r_f,
+    s_h,
+    r_h,
+    s_rim,
+    r_rim,
+    s_d,
+    r_d,
+    s_p,
+    r_p,
+    s_m,
+    r_m,
+    s_mx,
+    r_mx,
+    s_mr,
+    r_mr,
+    s_v,
+    r_v,
+    s_w,
+    r_w,
+    s_l,
+    r_l,
+):
+    me = lax.axis_index("sp")
+    member = lax.axis_index("tp")
+    seat = lax.rem(member, 2)
+    line = lax.div(member, 2)
+    sibling = member + 1 - 2 * seat
+    other = lax.rem(member + 2, groups)
+    tokens, width = out_grad.shape
+    slots = rows.shape[1]
+    ff = dn.shape[0]
+    share = width // groups
+    deep = n // 2
+    per = n // groups
+    span = width // n
+
+    barrier = pltpu.get_barrier_semaphore()
+
+    def call(off, carry):
+        pl.semaphore_signal(
+            barrier,
+            inc=1,
+            device_id={"sp": lax.rem(me + off, n)},
+            device_id_type=pl.DeviceIdType.MESH,
+        )
+        return carry
+
+    lax.fori_loop(1, n, call, 0)
+    for peer in (sibling, other):
+        pl.semaphore_signal(
+            barrier, inc=1, device_id={"tp": peer}, device_id_type=pl.DeviceIdType.MESH
+        )
+    loads = [
+        pltpu.make_async_copy(wg_hbm, wgu.at[:, pl.ds(0, ff)], load_sem.at[0]),
+        pltpu.make_async_copy(wu_hbm, wgu.at[:, pl.ds(ff, ff)], load_sem.at[1]),
+        pltpu.make_async_copy(rows_hbm, rows, load_sem.at[2]),
+        pltpu.make_async_copy(dn_hbm, dn, load_sem.at[3]),
+        pltpu.make_async_copy(ow_hbm, ow, load_sem.at[4]),
+    ]
+    for load in loads:
+        load.start()
+
+    def shift(k, way):
+        q = lax.div(k, 2)
+        step = lax.div(q + 1, 2) * (2 * lax.rem(q, 2) - 1) * way
+        deeper = lax.rem(lax.div(me, 2) + step + deep, deep)
+        side = lax.rem(lax.rem(me, 2) + lax.rem(k, 2), 2)
+        return 2 * deeper + side
+
+    def dest(k):
+        return shift(k, 1)
+
+    def source(k):
+        return shift(k, -1)
+
+    def slice_at(j):
+        return pl.ds(pl.multiple_of(j * span, span), span)
+
+    def across(k):
+        return remote(
+            send.at[dest(k)],
+            grads.at[me, :, columns(member, share)],
+            s_a.at[k],
+            r_a.at[k],
+            sp=dest(k),
+        )
+
+    def hand(k):
+        piece = grads.at[source(k), :, columns(member, share)]
+        return remote(piece, piece, s_b.at[k], r_b.at[k], tp=sibling)
+
+    def cross(k):
+        piece = grads.at[source(k), :, columns(member, share)]
+        return remote(piece, piece, s_x.at[k], r_x.at[k], tp=other)
+
+    def relay(k):
+        piece = grads.at[source(k), :, columns(other, share)]
+        return remote(piece, piece, s_g.at[k], r_g.at[k], tp=sibling)
+
+    def to_sibling(k, h):
+        return remote(
+            row_part.at[source(k), :, columns(2 * h + 1 - seat, share)],
+            near.at[source(k), h],
+            s_n.at[h, k],
+            r_n.at[h, k],
+            tp=sibling,
+        )
+
+    def to_other(k):
+        return remote(
+            pair.at[source(k), 1 - line], far.at[source(k)], s_f.at[k], r_f.at[k], tp=other
+        )
+
+    def to_home(k):
+        return remote(final.at[source(k)], back.at[me], s_h.at[k], r_h.at[k], sp=source(k))
+
+    def rim_copy(i, ref):
+        return remote(
+            ref.at[pl.ds(tokens - 16, 16)],
+            rim.at[i],
+            s_rim.at[i],
+            r_rim.at[i],
+            sp=lax.rem(me + 1, n),
+        )
+
+    def gated_along(q):
+        return remote(gated.at[me], gated.at[me], s_d.at[q], r_d.at[q], sp=dest(2 * q))
+
+    def gated_over(q):
+        piece = gated.at[source(2 * q)]
+        return remote(piece, piece, s_p.at[q], r_p.at[q], sp=dest(1))
+
+    names = lax.broadcasted_iota(jnp.int32, (n, tokens), 0)
+    chosen = jnp.zeros((n, tokens), jnp.bool_)
+    weights = jnp.zeros((n, tokens), F32)
+    for choice in range(routes.shape[0]):
+        named = names == routes[choice : choice + 1, :]
+        chosen = jnp.logical_or(chosen, named)
+        weights = weights + jnp.where(named, route_weight[choice : choice + 1, :], 0.0)
+    first = lax.broadcasted_iota(jnp.int32, (tokens, tokens), 0)
+    second = lax.broadcasted_iota(jnp.int32, (tokens, tokens), 1)
+    earlier = jnp.where(first < second, 1.0, 0.0).astype(BF16)
+    marks = jnp.where(chosen, 1.0, 0.0)
+    places = jnp.where(chosen, dot_nn(marks.astype(BF16), earlier), -1.0)
+    for e in range(n):
+        place[e] = places[e : e + 1, :]
+        weight[e] = weights[e : e + 1, :]
+    seats = lax.broadcasted_iota(jnp.int32, (slots, tokens), 0).astype(F32)
+
+    def pick(e):
+        filled = place[e] == seats
+        found = jnp.where(filled, 1.0, 0.0).astype(BF16)
+        picker[e] = found
+        held = jnp.sum(jnp.where(filled, weight[e], 0.0), axis=1, keepdims=True)
+        return found, held
+
+    pl.semaphore_wait(barrier, n + 1)
+    for i, ref in enumerate((in_gate, conv_input)):
+        rim_copy(i, ref).start()
+
+    def build(k, carry):
+        e = dest(k)
+        found, held = pick(e)
+        own = dot_nn(found, out_grad[:, columns(member, share)])
+        send[e] = (held * own).astype(BF16)
+        across(k).start()
+        return carry
+
+    lax.fori_loop(1, n, build, 0)
+    found, held = pick(me)
+    for g in range(groups):
+        at = pl.ds(g * share, share)
+        grads[me, :, at] = (held * dot_nn(found, out_grad[:, at])).astype(BF16)
+    for load in loads[:3]:
+        load.wait()
+    couples = 2
+
+    def project(c, carry):
+        at = pl.ds(c * couples, couples)
+        rows_c = rows[at].reshape(couples * slots, width)
+        hidden[at] = dot_nn(rows_c, wgu[...]).reshape(couples, slots, 2 * ff)
+        return carry
+
+    lax.fori_loop(0, n // couples, project, 0)
+
+    for i, ref in enumerate((in_gate, conv_input)):
+        rim_copy(i, ref).wait_recv()
+    prior = rim[0].astype(F32) * rim[1].astype(F32)
+    mixed[0:16] = jnp.where(me == 0, 0.0, prior)
+    mixed[pl.ds(16, tokens)] = in_gate[...].astype(F32) * conv_input[...].astype(F32)
+    reach = taps.shape[0]
+    conv_sum = taps[0:1, :] * mixed[pl.ds(16, tokens)]
+    for tap in range(1, reach):
+        conv_sum = conv_sum + taps[tap : tap + 1, :] * mixed[pl.ds(16 - tap, tokens)]
+    conv[...] = conv_sum
+    gated[me] = (out_gate[...].astype(F32) * conv_sum).astype(BF16)
+    for q in range(1, deep):
+        gated_along(q).start()
+    gated_over(0).start()
+    loads[3].wait()
+    loads[4].wait()
+
+    def arrive(k):
+        across(k).wait_recv()
+        cross(k).start()
+        hand(k).start()
+
+    def pass_on(k):
+        cross(k).wait_recv()
+        relay(k).start()
+
+    def backward(k):
+        @pl.when(k > 0)
+        def _():
+            hand(k).wait_recv()
+            relay(k).wait_recv()
+
+        s = source(k)
+        gate = hidden[s, :, 0:ff]
+        up = hidden[s, :, ff : 2 * ff]
+        sig = jax.nn.sigmoid(gate)
+        act[s] = (gate * sig * up).astype(BF16)
+        act_grad = dot_nt(grads[s], dn[...])
+        parts[s, :, 0:ff] = (act_grad * up * sig * (1.0 + gate * (1.0 - sig))).astype(BF16)
+        parts[s, :, ff : 2 * ff] = (act_grad * gate * sig).astype(BF16)
+        both = parts[s]
+        for g in range(groups):
+            at = pl.ds(g * share, share)
+            row_part[s, :, at] = dot_nt(both, wgu[at, :]).astype(BF16)
+        for h in range(2):
+            to_sibling(k, h).start()
+
+    def pair_up(k):
+        s = source(k)
+        for h in range(2):
+            to_sibling(k, h).wait_recv()
+            mine = row_part[s, :, columns(2 * h + seat, share)].astype(F32)
+            pair[s, h] = (mine + near[s, h].astype(F32)).astype(BF16)
+        to_other(k).start()
+
+    def finish(k):
+        s = source(k)
+        to_other(k).wait_recv()
+        final[s] = (pair[s, line].astype(F32) + far[s].astype(F32)).astype(BF16)
+
+        @pl.when(k > 0)
+        def _():
+            to_home(k).start()
+
+    def within(k, low, act_on):
+        @pl.when(jnp.logical_and(k >= low, k < n))
+        def _():
+            act_on(k)
+
+    def step(j, carry):
+        within(j + 1, 1, arrive)
+        within(j, 1, pass_on)
+        within(j - 1, 0, backward)
+        within(j - 2, 0, pair_up)
+        within(j - 3, 0, finish)
+        return carry
+
+    lax.fori_loop(0, n + 3, step, 0)
+
+    for q in range(1, deep):
+        gated_along(q).wait_recv()
+        gated_over(q).start()
+
+    total[...] = out_grad[:, columns(member, share)].astype(F32) + dot_tn(picker[me], final[me])
+
+    def gather_home(k, carry):
+        e = dest(k)
+        to_home(k).wait_recv()
+        total[...] += dot_tn(picker[e], back[e])
+        return carry
+
+    lax.fori_loop(1, n, gather_home, 0)
+    mid = total[...].astype(BF16)
+    mid_out[...] = mid
+    wide[:, columns(member, share)] = mid
+
+    def mid_sibling():
+        piece = wide.at[:, columns(member, share)]
+        return remote(piece, piece, s_m, r_m, tp=sibling)
+
+    def mid_other(q):
+        piece = wide.at[:, slice_at(member * per + q)]
+        return remote(piece, piece, s_mx.at[q], r_mx.at[q], tp=other)
+
+    def mid_relay(q):
+        piece = wide.at[:, slice_at(other * per + q)]
+        return remote(piece, piece, s_mr.at[q], r_mr.at[q], tp=sibling)
+
+    def slice_out(j):
+        return remote(wide.at[:, slice_at(j)], slices.at[me], s_v.at[j], r_v.at[me], sp=j)
+
+    def slice_in(s):
+        return remote(wide.at[:, slice_at(me)], slices.at[s], s_v.at[s], r_v.at[s], sp=s)
+
+    def slice_relay(s):
+        piece = slices.at[s]
+        return remote(piece, piece, s_w.at[s], r_w.at[s], tp=sibling)
+
+    def send_slice(j):
+        @pl.when(j != me)
+        def _():
+            slice_out(j).start()
+
+    for q in range(per):
+        mid_other(q).start()
+    mid_sibling().start()
+    for q in range(per):
+        send_slice(member * per + q)
+
+    chunk = 128 if width % 256 else 256
+    chunks = width // chunk
+
+    def weigh(piece, carry):
+        at = columns(piece, chunk)
+        tall = n * slots
+        grown = dot_tn(rows[:, :, at].reshape(tall, chunk), parts[...].reshape(tall, 2 * ff))
+        gate_out[at, :] = grown[:, 0:ff].astype(BF16)
+        up_out[at, :] = grown[:, ff : 2 * ff].astype(BF16)
+        down_out[:, at] = dot_tn(
+            act[...].reshape(tall, ff), grads[:, :, at].reshape(tall, chunk)
+        ).astype(BF16)
+        return carry
+
+    lax.fori_loop(0, chunks // 2, weigh, 0)
+    for q in range(per):
+        mid_other(q).wait_recv()
+        mid_relay(q).start()
+        send_slice(other * per + q)
+    lax.fori_loop(chunks // 2, chunks, weigh, 0)
+    mid_sibling().wait_recv()
+    for q in range(per):
+        mid_relay(q).wait_recv()
+    gated_grad = dot_nn(wide[...], ow[...])
+    conv_grad = gated_grad * out_gate[...].astype(F32)
+    follow[pl.ds(0, tokens)] = conv_grad
+
+    back_rim = remote(
+        follow.at[pl.ds(0, 8)], later, s_l, r_l, sp=lax.rem(me + n - 1, n)
+    )
+    back_rim.start()
+    out_gate_out[...] = (gated_grad * conv[...]).astype(BF16)
+    for q in range(deep):
+        gated_over(q).wait_recv()
+    weight_out[...] = dot_tn(wide[:, slice_at(me)], gated[me])
+    holder = lax.rem(lax.div(me, per), 2)
+
+    def meet(off, carry):
+        s = lax.rem(me + off, n)
+
+        @pl.when(holder == seat)
+        def _():
+            slice_in(s).wait_recv()
+            slice_relay(s).start()
+
+        @pl.when(holder != seat)
+        def _():
+            slice_relay(s).wait_recv()
+
+        weight_out[...] += dot_tn(slices[s], gated[s])
+        return carry
+
+    lax.fori_loop(1, n, meet, 0)
+    back_rim.wait_recv()
+    follow[pl.ds(tokens, 8)] = jnp.where(me == n - 1, 0.0, later[...])
+    mixed_grad = taps[0:1, :] * follow[pl.ds(0, tokens)]
+    for tap in range(1, reach):
+        mixed_grad = mixed_grad + taps[tap : tap + 1, :] * follow[pl.ds(tap, tokens)]
+    input_out[...] = (mixed_grad * in_gate[...].astype(F32)).astype(BF16)
+    in_gate_out[...] = (mixed_grad * conv_input[...].astype(F32)).astype(BF16)
+
+    def drain(k, carry):
+        @pl.when(k > 0)
+        def _():
+            across(k).wait_send()
+            hand(k).wait_send()
+            cross(k).wait_send()
+            relay(k).wait_send()
+            to_home(k).wait_send()
+
+        for h in range(2):
+            to_sibling(k, h).wait_send()
+        to_other(k).wait_send()
+        return carry
+
+    lax.fori_loop(0, n, drain, 0)
+
+    def drain_slices(off, carry):
+        s = lax.rem(me + off, n)
+
+        @pl.when(holder == seat)
+        def _():
+            slice_relay(s).wait_send()
+
+        return carry
+
+    lax.fori_loop(1, n, drain_slices, 0)
+    for i, ref in enumerate((in_gate, conv_input)):
+        rim_copy(i, ref).wait_send()
+    for q in range(deep):
+        gated_over(q).wait_send()
+        if q > 0:
+            gated_along(q).wait_send()
+    mid_sibling().wait_send()
+    back_rim.wait_send()
+    for q in range(per):
+        mid_other(q).wait_send()
+        mid_relay(q).wait_send()
+        for owner in (member, other):
+
+            @pl.when(owner * per + q != me)
+            def _():
+                slice_out(owner * per + q).wait_send()
+
+
+def fused(
+    out_grad,
+    routes,
+    route_weight,
+    rows,
+    gate_weight,
+    up_weight,
+    down_weight,
+    conv_input,
+    out_gate,
+    in_gate,
+    taps,
+    out_weight,
+    groups,
+):
+    n, slots, width = rows.shape
+    tokens = out_grad.shape[0]
+    ff = gate_weight.shape[1]
+    chans = conv_input.shape[1]
+    share, span, deep, per = width // groups, width // n, n // 2, n // groups
+    dma = pltpu.SemaphoreType.DMA
+
+    def held(*shape):
+        return pltpu.VMEM(shape, BF16)
+
+    def exact(*shape):
+        return pltpu.VMEM(shape, F32)
+
+    small = jax.ShapeDtypeStruct((tokens, chans), BF16)
+    return pl.pallas_call(
+        functools.partial(fused_kernel, n, groups),
+        out_shape=(
+            jax.ShapeDtypeStruct((width, ff), BF16),
+            jax.ShapeDtypeStruct((width, ff), BF16),
+            jax.ShapeDtypeStruct((ff, width), BF16),
+            jax.ShapeDtypeStruct((tokens, share), BF16),
+            jax.ShapeDtypeStruct((span, chans), F32),
+            small,
+            small,
+            small,
+        ),
+        in_specs=[VMEM_SPEC] * 7 + [ANY_SPEC] * 5,
+        out_specs=(VMEM_SPEC,) * 8,
+        scratch_shapes=[
+            held(n, slots, width),
+            held(width, 2 * ff),
+            held(ff, width),
+            held(width, chans),
+            exact(n, slots, 2 * ff),
+            exact(n, 1, tokens),
+            exact(n, 1, tokens),
+            held(n, slots, tokens),
+            held(n, slots, share),
+            held(n, slots, width),
+            held(n, slots, ff),
+            held(n, slots, 2 * ff),
+            held(n, slots, width),
+            held(n, 2, slots, share),
+            held(n, 2, slots, share),
+            held(n, slots, share),
+            held(n, slots, share),
+            held(n, slots, share),
+            exact(tokens, share),
+            held(tokens, width),
+            held(2, 16, chans),
+            exact(16 + tokens, chans),
+            exact(tokens, chans),
+            held(n, tokens, chans),
+            held(n, tokens, span),
+            exact(tokens + 8, chans),
+            exact(8, chans),
+            dma((5,)),
+        ]
+        + [dma((n,))] * 8
+        + [dma((2, n))] * 2
+        + [dma((n,))] * 4
+        + [dma((2,))] * 2
+        + [dma((deep,))] * 4
+        + [dma(())] * 2
+        + [dma((per,))] * 4
+        + [dma((n,))] * 4
+        + [dma(())] * 2,
+        compiler_params=pltpu.CompilerParams(collective_id=4, has_side_effects=True),
+    )(
+        out_grad,
+        routes.T,
+        route_weight.T,
+        conv_input,
+        out_gate,
+        in_gate,
+        taps,
+        rows,
+        gate_weight,
+        up_weight,
+        down_weight,
+        out_weight,
+    )
+
+
+def fits_fused(tokens, slots, width, sources, groups):
+    tidy = slots % 16 == 0 and tokens % 16 == 0 and width % (128 * sources) == 0
+    return tidy and groups == 4 and sources % 4 == 0
+
+
 def on_device(
+    out_grad,
+    routes,
+    route_weight,
+    expert_rows,
+    gate_weight,
+    up_weight,
+    down_weight,
+    conv_input,
+    out_gate,
+    in_gate,
+    taps,
+    out_weight,
+):
+    groups = lax.axis_size("tp")
+    sources = lax.axis_size("sp")
+    slots, width = expert_rows.shape[2:]
+    assert gate_weight.shape[0] == 1
+    if not fits_fused(out_grad.shape[0], slots, width, sources, groups):
+        return staged(
+            out_grad,
+            routes,
+            route_weight,
+            expert_rows,
+            gate_weight,
+            up_weight,
+            down_weight,
+            conv_input,
+            out_gate,
+            in_gate,
+            taps,
+            out_weight,
+        )
+    outs = fused(
+        out_grad,
+        routes,
+        route_weight,
+        expert_rows.reshape(sources, slots, width),
+        gate_weight[0],
+        up_weight[0],
+        down_weight[0],
+        conv_input,
+        out_gate,
+        in_gate,
+        taps,
+        out_weight,
+        groups,
+    )
+    return tuple(out[None] for out in outs[:3]) + tuple(outs[3:])
+
+
+def staged(
     out_grad,
     routes,
     route_weight,

time: 140 us -> 82.4 us (0.59); the launches traced: 138 us -> 82.2 us
  Pallas kernels: 102 us -> 72.5 us
  matrix products: 17.6 us -> 0 us
  starting transfers between devices: 5.24 us -> 0 us
  other arithmetic: 4.61 us -> 0 us
    pallas_call x4 -> x1, Pallas kernels: 102 us -> 72.5 us  [fused(): pl.pallas_call(functools.partial(fused_kernel, n, groups), out_shape=(jax...]
    dot_general x8 -> x0, matrix products: 17.6 us -> none  [the longest x1 4.38 us: on_device(): lax.dot_general(grads, tall_down, (((1,), (1,)), ((), ())), preferred_ele...]
    ppermute x2 -> x0, starting transfers between devices: 5.24 us -> none  [passed_along(): return lax.ppermute(shard, axis, pairs)]
    unnamed x30 -> x20, local copies, waits for them, and re-layouts: 5.47 us -> 8.97 us
  transfers between devices with their start and end apart: 2 -> 0, of which waited for: 0 -> 0; matrix products, arithmetic and copies ran while one was open for 14% -> 0% of each run, Pallas kernels for 74% -> 0%
where the time goes in v1:
time: 82.4 us; the launch traced here: 82.2 us
  Pallas kernels  72.5 us (88%)
  local copies, waits for them, and re-layouts  8.97 us (11%)
    pallas_call x1, Pallas kernels, fused(): pl.pallas_call(functools.partial(fused_kernel, n, groups), out_shape=(jax...  72.5 us
    unnamed x20, local copies, waits for them, and re-layouts  8.97 us

profile of v1, /device:TPU:1, one launch (start us, length us, event | category | flops | bytes accessed | tf_op | source)
XLA Modules:
  0.0 82.2 jit_solution(1172102885549461765)
XLA Ops:
  0.6 72.5 %shard_map.179 = (bf16[2048,256]{1,0:T(8,128)(2,1)}, bf16[2048,256]{1,0:T(8,128)(2,1)}, bf16[256,2048]{1,0:T(8,128)(2,1)}, bf16[192,512]{1,0:T(8,128)(2,1)}, f32...) custom-call(bf16[192,2048]{1,0:T(8,128)(2,1)} %out_grad.1, ...), custom_call_target="tpu_custom_call" | custom-call | tf_op jit(solution)/shard_map/pallas_call | solution.py:1066
  73.2 0.0 copy-start
  73.2 0.0 copy-start.2
  73.2 0.0 copy-start.1
  73.2 0.0 copy-start.5
  73.2 2.4 %copy.28 = bf16[1,2048,256]{2,1,0:T(8,128)(2,1)} copy(bf16[1,2048,256]{2,1,0:T(8,128)(2,1)} %bitcast.15) | data formatting | bytes 2097152
  75.6 0.0 copy-start.4
  75.6 0.0 copy-start.3
  75.6 2.3 %copy.29 = bf16[1,2048,256]{2,1,0:T(8,128)(2,1)} copy(bf16[1,2048,256]{2,1,0:T(8,128)(2,1)} %bitcast.14) | data formatting | bytes 2097152
  77.9 0.0 copy-done
  77.9 1.0 %copy.30 = bf16[1,256,2048]{2,1,0:T(8,128)(2,1)} copy(bf16[1,256,2048]{2,1,0:T(8,128)(2,1)S(1)} %bitcast.13) | data formatting | bytes 2097152
  78.9 0.0 copy-done.2
  78.9 0.7 copy.31
  79.6 0.0 copy-done.1
  79.6 0.7 copy.32
  80.3 0.0 copy-done.5
  80.3 0.6 copy.33
  80.9 0.0 copy-done.4
  80.9 0.6 copy.34
  81.6 0.0 copy-done.3
  81.6 0.6 copy.35
Async XLA Ops:
  73.2 4.7 %copy-start = (bf16[256,2048]{1,0:T(8,128)(2,1)S(1)}, bf16[256,2048]{1,0:T(8,128)(2,1)}, u32[]{:S(2)}) copy-start(bf16[256,2048]{1,0:T(8,128)(2,1)} %get-tuple-element.18) | copy-start | bytes 3145732
  73.2 5.7 %copy-start.2 = (bf16[192,512]{1,0:T(8,128)(2,1)S(1)}, bf16[192,512]{1,0:T(8,128)(2,1)}, u32[]{:S(2)}) copy-start(bf16[192,512]{1,0:T(8,128)(2,1)} %get-tuple-element.35) | copy-start | bytes 589828
  73.2 6.4 %copy-start.1 = (f32[256,256]{1,0:T(8,128)S(1)}, f32[256,256]{1,0:T(8,128)}, u32[]{:S(2)}) copy-start(f32[256,256]{1,0:T(8,128)} %get-tuple-element.36) | copy-start | bytes 786436
  73.2 7.1 %copy-start.5 = (bf16[192,256]{1,0:T(8,128)(2,1)S(1)}, bf16[192,256]{1,0:T(8,128)(2,1)}, u32[]{:S(2)}) copy-start(bf16[192,256]{1,0:T(8,128)(2,1)} %get-tuple-element.37) | copy-start | bytes 294916
  75.6 5.3 %copy-start.4 = (bf16[192,256]{1,0:T(8,128)(2,1)S(1)}, bf16[192,256]{1,0:T(8,128)(2,1)}, u32[]{:S(2)}) copy-start(bf16[192,256]{1,0:T(8,128)(2,1)} %get-tuple-element.38) | copy-start | bytes 294916
  75.6 6.0 %copy-start.3 = (bf16[192,256]{1,0:T(8,128)(2,1)S(1)}, bf16[192,256]{1,0:T(8,128)(2,1)}, u32[]{:S(2)}) copy-start(bf16[192,256]{1,0:T(8,128)(2,1)} %get-tuple-element.39) | copy-start | bytes 294916

commit v2 on v1

--- a/solution.py
+++ b/solution.py
@@ -538,6 +538,7 @@
     )(parts)
 
 
+HBM_SPEC = pl.BlockSpec(memory_space=pltpu.HBM)
 BF16, F32 = jnp.bfloat16, jnp.float32
 
 
@@ -556,13 +557,13 @@
 def fused_kernel(
     n,
     groups,
-    out_grad,
-    routes,
-    route_weight,
-    conv_input,
-    out_gate,
-    in_gate,
-    taps,
+    out_grad_hbm,
+    routes_hbm,
+    route_weight_hbm,
+    conv_input_hbm,
+    out_gate_hbm,
+    in_gate_hbm,
+    taps_hbm,
     rows_hbm,
     wg_hbm,
     wu_hbm,
@@ -576,6 +577,13 @@
     input_out,
     out_gate_out,
     in_gate_out,
+    out_grad,
+    routes,
+    route_weight,
+    conv_input,
+    out_gate,
+    in_gate,
+    taps,
     rows,
     wgu,
     dn,
@@ -667,6 +675,15 @@
         pl.semaphore_signal(
             barrier, inc=1, device_id={"tp": peer}, device_id_type=pl.DeviceIdType.MESH
         )
+    early = [
+        pltpu.make_async_copy(routes_hbm, routes, load_sem.at[5]),
+        pltpu.make_async_copy(route_weight_hbm, route_weight, load_sem.at[6]),
+        pltpu.make_async_copy(out_grad_hbm, out_grad, load_sem.at[7]),
+        pltpu.make_async_copy(in_gate_hbm, in_gate, load_sem.at[8]),
+        pltpu.make_async_copy(conv_input_hbm, conv_input, load_sem.at[9]),
+        pltpu.make_async_copy(out_gate_hbm, out_gate, load_sem.at[10]),
+        pltpu.make_async_copy(taps_hbm, taps, load_sem.at[11]),
+    ]
     loads = [
         pltpu.make_async_copy(wg_hbm, wgu.at[:, pl.ds(0, ff)], load_sem.at[0]),
         pltpu.make_async_copy(wu_hbm, wgu.at[:, pl.ds(ff, ff)], load_sem.at[1]),
@@ -674,7 +691,7 @@
         pltpu.make_async_copy(dn_hbm, dn, load_sem.at[3]),
         pltpu.make_async_copy(ow_hbm, ow, load_sem.at[4]),
     ]
-    for load in loads:
+    for load in early + loads:
         load.start()
 
     def shift(k, way):
@@ -747,6 +764,8 @@
         piece = gated.at[source(2 * q)]
         return remote(piece, piece, s_p.at[q], r_p.at[q], sp=dest(1))
 
+    for load in early[:2]:
+        load.wait()
     names = lax.broadcasted_iota(jnp.int32, (n, tokens), 0)
     chosen = jnp.zeros((n, tokens), jnp.bool_)
     weights = jnp.zeros((n, tokens), F32)
@@ -771,6 +790,8 @@
         held = jnp.sum(jnp.where(filled, weight[e], 0.0), axis=1, keepdims=True)
         return found, held
 
+    for load in early[2:]:
+        load.wait()
     pl.semaphore_wait(barrier, n + 1)
     for i, ref in enumerate((in_gate, conv_input)):
         rim_copy(i, ref).start()
@@ -1032,6 +1053,27 @@
             @pl.when(owner * per + q != me)
             def _():
                 slice_out(owner * per + q).wait_send()
+
+
+def settle_kernel(count, *refs):
+    sources, targets, sem = refs[:count], refs[count : 2 * count], refs[2 * count]
+    moves = [pltpu.make_async_copy(a, b, sem.at[i]) for i, (a, b) in enumerate(zip(sources, targets))]
+    for move in moves:
+        move.start()
+    for move in moves:
+        move.wait()
+
+
+def settle(arrays):
+    count = len(arrays)
+    return pl.pallas_call(
+        functools.partial(settle_kernel, count),
+        out_shape=tuple(jax.ShapeDtypeStruct(a.shape, a.dtype) for a in arrays),
+        in_specs=[ANY_SPEC] * count,
+        out_specs=(HBM_SPEC,) * count,
+        scratch_shapes=[pltpu.SemaphoreType.DMA((count,))],
+        compiler_params=pltpu.CompilerParams(vmem_limit_bytes=2**20),
+    )(*arrays)
 
 
 def fused(
@@ -1062,22 +1104,43 @@
     def exact(*shape):
         return pltpu.VMEM(shape, F32)
 
-    small = jax.ShapeDtypeStruct((tokens, chans), BF16)
+    operands = (
+        out_grad,
+        routes.T,
+        route_weight.T,
+        conv_input,
+        out_gate,
+        in_gate,
+        taps,
+        rows,
+        gate_weight,
+        up_weight,
+        down_weight,
+        out_weight,
+    )
+    small = held(tokens, chans)
     return pl.pallas_call(
         functools.partial(fused_kernel, n, groups),
         out_shape=(
-            jax.ShapeDtypeStruct((width, ff), BF16),
-            jax.ShapeDtypeStruct((width, ff), BF16),
-            jax.ShapeDtypeStruct((ff, width), BF16),
-            jax.ShapeDtypeStruct((tokens, share), BF16),
-            jax.ShapeDtypeStruct((span, chans), F32),
+            held(width, ff),
+            held(width, ff),
+            held(ff, width),
+            held(tokens, share),
+            exact(span, chans),
             small,
             small,
             small,
         ),
-        in_specs=[VMEM_SPEC] * 7 + [ANY_SPEC] * 5,
+        in_specs=[HBM_SPEC] * 12,
         out_specs=(VMEM_SPEC,) * 8,
         scratch_shapes=[
+            held(tokens, width),
+            pltpu.VMEM(routes.T.shape, routes.dtype),
+            exact(*route_weight.T.shape),
+            held(tokens, chans),
+            held(tokens, chans),
+            held(tokens, chans),
+            exact(*taps.shape),
             held(n, slots, width),
             held(width, 2 * ff),
             held(ff, width),
@@ -1105,7 +1168,7 @@
             held(n, tokens, span),
             exact(tokens + 8, chans),
             exact(8, chans),
-            dma((5,)),
+            dma((12,)),
         ]
         + [dma((n,))] * 8
         + [dma((2, n))] * 2
@@ -1116,21 +1179,10 @@
         + [dma((per,))] * 4
         + [dma((n,))] * 4
         + [dma(())] * 2,
-        compiler_params=pltpu.CompilerParams(collective_id=4, has_side_effects=True),
-    )(
-        out_grad,
-        routes.T,
-        route_weight.T,
-        conv_input,
-        out_gate,
-        in_gate,
-        taps,
-        rows,
-        gate_weight,
-        up_weight,
-        down_weight,
-        out_weight,
-    )
+        compiler_params=pltpu.CompilerParams(
+            collective_id=4, has_side_effects=True, vmem_limit_bytes=40 * 2**20
+        ),
+    )(*(pltpu.with_memory_space_constraint(a, pltpu.HBM) for a in operands))
 
 
 def fits_fused(tokens, slots, width, sources, groups):
@@ -1186,6 +1238,7 @@
         out_weight,
         groups,
     )
+    outs = settle(outs)
     return tuple(out[None] for out in outs[:3]) + tuple(outs[3:])
 
 

time: 82.4 us -> 72 us (0.87)
  local copies, waits for them, and re-layouts: 8.97 us -> 0 us
  Pallas kernels: 72.5 us -> 71.1 us
    unnamed x20 -> x0, local copies, waits for them, and re-layouts: 8.97 us -> none
    pallas_call x1 -> x2, Pallas kernels: 72.5 us -> 71.1 us  [the longest x1 69.2 us: fused(): pl.pallas_call(functools.partial(fused_kernel, n, groups), out_shape=(hel...]
where the time goes in v2:
time: 72 us; the launch traced here: 71.8 us
  Pallas kernels  71.1 us (99%)
    pallas_call x1, Pallas kernels, fused(): pl.pallas_call(functools.partial(fused_kernel, n, groups), out_shape=(hel...  69.2 us
    pallas_call x1, Pallas kernels, settle(): pl.pallas_call(functools.partial(settle_kernel, count), out_shape=tuple((...  1.97 us

profile of v2, /device:TPU:1, one launch (start us, length us, event | category | flops | bytes accessed | tf_op | source)
XLA Modules:
  0.0 71.8 jit_solution(16448816667339837976)
XLA Ops:
  0.6 69.2 %shard_map.179 = (bf16[2048,256]{1,0:T(8,128)(2,1)S(1)}, bf16[2048,256]{1,0:T(8,128)(2,1)S(1)}, bf16[256,2048]{1,0:T(8,128)(2,1)S(1)}, bf16[192,512]{1,0:T(8,128...) custom-call(bf16[192,2048]{1,0:T(8,128)(2,1)} %out_grad_hbm.1, ...), custom_call_target="tpu_custom_call" | custom-call | tf_op jit(solution)/shard_map/pallas_call | solution.py:1122
  69.8 2.0 %shard_map.180 = (bf16[2048,256]{1,0:T(8,128)(2,1)}, bf16[2048,256]{1,0:T(8,128)(2,1)}, bf16[256,2048]{1,0:T(8,128)(2,1)}, bf16[192,512]{1,0:T(8,128)(2,1)}, f32...) custom-call(bf16[2048,256]{1,0:T(8,128)(2,1)S(1)} %get-tuple-element.24.refs_0_, ...), custom_call_target="tpu_custom_call" | custom-call | tf_op jit(solution)/shard_map/pallas_call | solution.py:1069

commit v3 on v2

--- a/solution.py
+++ b/solution.py
@@ -611,6 +611,12 @@
     slices,
     follow,
     later,
+    far_routes,
+    far_weight,
+    far_tokens,
+    far_total,
+    sum_out,
+    sum_in,
     load_sem,
     s_a,
     r_a,
@@ -632,6 +638,12 @@
     r_d,
     s_p,
     r_p,
+    s_c,
+    r_c,
+    s_e,
+    r_e,
+    s_t,
+    r_t,
     s_m,
     r_m,
     s_mx,
@@ -655,7 +667,8 @@
     slots = rows.shape[1]
     ff = dn.shape[0]
     share = width // groups
-    deep = n // 2
+    team = n // 2
+    pace = team // 2
     per = n // groups
     span = width // n
 
@@ -694,29 +707,33 @@
     for load in early + loads:
         load.start()
 
-    def shift(k, way):
-        q = lax.div(k, 2)
-        step = lax.div(q + 1, 2) * (2 * lax.rem(q, 2) - 1) * way
-        deeper = lax.rem(lax.div(me, 2) + step + deep, deep)
-        side = lax.rem(lax.rem(me, 2) + lax.rem(k, 2), 2)
-        return 2 * deeper + side
-
-    def dest(k):
-        return shift(k, 1)
+    spot = lax.rem(me, team)
+    base = me - spot
+    mirror = lax.rem(me + team, n)
+    partner = me + 1 - 2 * lax.rem(me, 2)
+
+    def taker(k):
+        return base + lax.rem(spot + lax.rem(k, team), team)
+
+    def giver(k):
+        return base + lax.rem(spot + team - lax.rem(k, team), team)
 
     def source(k):
-        return shift(k, -1)
+        return lax.rem(giver(k) + team * lax.div(k, team), n)
+
+    def owner(k):
+        return lax.rem(me + team * lax.div(k, team), n)
 
     def slice_at(j):
         return pl.ds(pl.multiple_of(j * span, span), span)
 
     def across(k):
         return remote(
-            send.at[dest(k)],
-            grads.at[me, :, columns(member, share)],
+            send.at[k],
+            grads.at[owner(k), :, columns(member, share)],
             s_a.at[k],
             r_a.at[k],
-            sp=dest(k),
+            sp=taker(k),
         )
 
     def hand(k):
@@ -746,7 +763,12 @@
         )
 
     def to_home(k):
-        return remote(final.at[source(k)], back.at[me], s_h.at[k], r_h.at[k], sp=source(k))
+        return remote(final.at[source(k)], back.at[k], s_h.at[k], r_h.at[k], sp=giver(k))
+
+    def to_mirror(i):
+        sources = (routes, route_weight, out_grad.at[:, columns(member, share)], sum_out)
+        landings = (far_routes, far_weight, far_tokens, sum_in)
+        return remote(sources[i], landings[i], s_t.at[i], r_t.at[i], sp=mirror)
 
     def rim_copy(i, ref):
         return remote(
@@ -758,54 +780,73 @@
         )
 
     def gated_along(q):
-        return remote(gated.at[me], gated.at[me], s_d.at[q], r_d.at[q], sp=dest(2 * q))
+        return remote(gated.at[me], gated.at[me], s_d.at[q], r_d.at[q], sp=taker(2 * q))
+
+    def gated_across():
+        return remote(gated.at[me], gated.at[me], s_c, r_c, sp=mirror)
+
+    def gated_on(q):
+        piece = gated.at[mirror]
+        return remote(piece, piece, s_e.at[q], r_e.at[q], sp=taker(2 * q))
 
     def gated_over(q):
         piece = gated.at[source(2 * q)]
-        return remote(piece, piece, s_p.at[q], r_p.at[q], sp=dest(1))
+        return remote(piece, piece, s_p.at[q], r_p.at[q], sp=partner)
 
     for load in early[:2]:
         load.wait()
-    names = lax.broadcasted_iota(jnp.int32, (n, tokens), 0)
-    chosen = jnp.zeros((n, tokens), jnp.bool_)
-    weights = jnp.zeros((n, tokens), F32)
-    for choice in range(routes.shape[0]):
-        named = names == routes[choice : choice + 1, :]
-        chosen = jnp.logical_or(chosen, named)
-        weights = weights + jnp.where(named, route_weight[choice : choice + 1, :], 0.0)
     first = lax.broadcasted_iota(jnp.int32, (tokens, tokens), 0)
     second = lax.broadcasted_iota(jnp.int32, (tokens, tokens), 1)
     earlier = jnp.where(first < second, 1.0, 0.0).astype(BF16)
-    marks = jnp.where(chosen, 1.0, 0.0)
-    places = jnp.where(chosen, dot_nn(marks.astype(BF16), earlier), -1.0)
-    for e in range(n):
-        place[e] = places[e : e + 1, :]
-        weight[e] = weights[e : e + 1, :]
     seats = lax.broadcasted_iota(jnp.int32, (slots, tokens), 0).astype(F32)
 
-    def pick(e):
+    def settle_places(named_by, weighed_by):
+        names = lax.broadcasted_iota(jnp.int32, (n, tokens), 0)
+        chosen = jnp.zeros((n, tokens), jnp.bool_)
+        weights = jnp.zeros((n, tokens), F32)
+        for choice in range(routes.shape[0]):
+            named = names == named_by[choice : choice + 1, :]
+            chosen = jnp.logical_or(chosen, named)
+            weights = weights + jnp.where(named, weighed_by[choice : choice + 1, :], 0.0)
+        marks = jnp.where(chosen, 1.0, 0.0)
+        places = jnp.where(chosen, dot_nn(marks.astype(BF16), earlier), -1.0)
+        for e in range(n):
+            place[e] = places[e : e + 1, :]
+            weight[e] = weights[e : e + 1, :]
+
+    def pick(k):
+        e = taker(k)
         filled = place[e] == seats
         found = jnp.where(filled, 1.0, 0.0).astype(BF16)
-        picker[e] = found
+        picker[k] = found
         held = jnp.sum(jnp.where(filled, weight[e], 0.0), axis=1, keepdims=True)
         return found, held
 
+    settle_places(routes, route_weight)
     for load in early[2:]:
         load.wait()
     pl.semaphore_wait(barrier, n + 1)
     for i, ref in enumerate((in_gate, conv_input)):
         rim_copy(i, ref).start()
 
+    for i in range(3):
+        to_mirror(i).start()
+
     def build(k, carry):
-        e = dest(k)
-        found, held = pick(e)
+        found, held = pick(k)
         own = dot_nn(found, out_grad[:, columns(member, share)])
-        send[e] = (held * own).astype(BF16)
+        send[k] = (held * own).astype(BF16)
         across(k).start()
         return carry
 
-    lax.fori_loop(1, n, build, 0)
-    found, held = pick(me)
+    def build_far(k, carry):
+        found, held = pick(k)
+        send[k] = (held * dot_nn(found, far_tokens[...])).astype(BF16)
+        across(k).start()
+        return carry
+
+    lax.fori_loop(1, team, build, 0)
+    found, held = pick(0)
     for g in range(groups):
         at = pl.ds(g * share, share)
         grads[me, :, at] = (held * dot_nn(found, out_grad[:, at])).astype(BF16)
@@ -832,14 +873,28 @@
         conv_sum = conv_sum + taps[tap : tap + 1, :] * mixed[pl.ds(16 - tap, tokens)]
     conv[...] = conv_sum
     gated[me] = (out_gate[...].astype(F32) * conv_sum).astype(BF16)
-    for q in range(1, deep):
+    for q in range(1, pace):
         gated_along(q).start()
+    gated_across().start()
     gated_over(0).start()
     loads[3].wait()
     loads[4].wait()
 
+    def serve():
+        for i in range(3):
+            to_mirror(i).wait_recv()
+        settle_places(far_routes, far_weight)
+        lax.fori_loop(team + 1, n, build_far, 0)
+        found, held = pick(team)
+        grads[mirror, :, columns(member, share)] = (
+            held * dot_nn(found, far_tokens[...])
+        ).astype(BF16)
+
     def arrive(k):
-        across(k).wait_recv()
+        @pl.when(k != team)
+        def _():
+            across(k).wait_recv()
+
         cross(k).start()
         hand(k).start()
 
@@ -881,16 +936,37 @@
         to_other(k).wait_recv()
         final[s] = (pair[s, line].astype(F32) + far[s].astype(F32)).astype(BF16)
 
-        @pl.when(k > 0)
+        @pl.when(lax.rem(k, team) > 0)
         def _():
             to_home(k).start()
 
-    def within(k, low, act_on):
-        @pl.when(jnp.logical_and(k >= low, k < n))
+    def within(p, low, act_on):
+        k = jnp.where(p < team - 1, p, jnp.where(p < n - 1, p + 1, team - 1))
+
+        @pl.when(jnp.logical_and(p >= low, p < n))
         def _():
             act_on(k)
 
     def step(j, carry):
+        @pl.when(j == team - 2)
+        def _():
+            serve()
+
+        @pl.when(j == team - 1)
+        def _():
+            gated_across().wait_recv()
+            for q in range(1, pace):
+                gated_on(q).start()
+                gated_along(q).wait_recv()
+                gated_over(q).start()
+            gated_over(pace).start()
+
+        @pl.when(j == n - 1)
+        def _():
+            for q in range(1, pace):
+                gated_on(q).wait_recv()
+                gated_over(pace + q).start()
+
         within(j + 1, 1, arrive)
         within(j, 1, pass_on)
         within(j - 1, 0, backward)
@@ -900,20 +976,27 @@
 
     lax.fori_loop(0, n + 3, step, 0)
 
-    for q in range(1, deep):
-        gated_along(q).wait_recv()
-        gated_over(q).start()
-
-    total[...] = out_grad[:, columns(member, share)].astype(F32) + dot_tn(picker[me], final[me])
+    far_total[...] = dot_tn(picker[team], final[mirror])
+
+    def gather_far(k, carry):
+        to_home(k).wait_recv()
+        far_total[...] += dot_tn(picker[k], back[k])
+        return carry
+
+    lax.fori_loop(team + 1, n, gather_far, 0)
+    sum_out[...] = far_total[...].astype(BF16)
+    to_mirror(3).start()
+
+    total[...] = out_grad[:, columns(member, share)].astype(F32) + dot_tn(picker[0], final[me])
 
     def gather_home(k, carry):
-        e = dest(k)
         to_home(k).wait_recv()
-        total[...] += dot_tn(picker[e], back[e])
-        return carry
-
-    lax.fori_loop(1, n, gather_home, 0)
-    mid = total[...].astype(BF16)
+        total[...] += dot_tn(picker[k], back[k])
+        return carry
+
+    lax.fori_loop(1, team, gather_home, 0)
+    to_mirror(3).wait_recv()
+    mid = (total[...] + sum_in[...].astype(F32)).astype(BF16)
     mid_out[...] = mid
     wide[:, columns(member, share)] = mid
 
@@ -982,7 +1065,7 @@
     )
     back_rim.start()
     out_gate_out[...] = (gated_grad * conv[...]).astype(BF16)
-    for q in range(deep):
+    for q in range(team):
         gated_over(q).wait_recv()
     weight_out[...] = dot_tn(wide[:, slice_at(me)], gated[me])
     holder = lax.rem(lax.div(me, per), 2)
@@ -1012,13 +1095,16 @@
     in_gate_out[...] = (mixed_grad * conv_input[...].astype(F32)).astype(BF16)
 
     def drain(k, carry):
+        @pl.when(lax.rem(k, team) > 0)
+        def _():
+            across(k).wait_send()
+            to_home(k).wait_send()
+
         @pl.when(k > 0)
         def _():
-            across(k).wait_send()
             hand(k).wait_send()
             cross(k).wait_send()
             relay(k).wait_send()
-            to_home(k).wait_send()
 
         for h in range(2):
             to_sibling(k, h).wait_send()
@@ -1039,10 +1125,14 @@
     lax.fori_loop(1, n, drain_slices, 0)
     for i, ref in enumerate((in_gate, conv_input)):
         rim_copy(i, ref).wait_send()
-    for q in range(deep):
+    for q in range(team):
         gated_over(q).wait_send()
-        if q > 0:
-            gated_along(q).wait_send()
+    for q in range(1, pace):
+        gated_along(q).wait_send()
+        gated_on(q).wait_send()
+    gated_across().wait_send()
+    for i in range(4):
+        to_mirror(i).wait_send()
     mid_sibling().wait_send()
     back_rim.wait_send()
     for q in range(per):
@@ -1095,7 +1185,7 @@
     tokens = out_grad.shape[0]
     ff = gate_weight.shape[1]
     chans = conv_input.shape[1]
-    share, span, deep, per = width // groups, width // n, n // 2, n // groups
+    share, span, team, per = width // groups, width // n, n // 2, n // groups
     dma = pltpu.SemaphoreType.DMA
 
     def held(*shape):
@@ -1168,13 +1258,22 @@
             held(n, tokens, span),
             exact(tokens + 8, chans),
             exact(8, chans),
+            pltpu.VMEM(routes.T.shape, routes.dtype),
+            exact(*route_weight.T.shape),
+            held(tokens, share),
+            exact(tokens, share),
+            held(tokens, share),
+            held(tokens, share),
             dma((12,)),
         ]
         + [dma((n,))] * 8
         + [dma((2, n))] * 2
         + [dma((n,))] * 4
         + [dma((2,))] * 2
-        + [dma((deep,))] * 4
+        + [dma((team,))] * 4
+        + [dma(())] * 2
+        + [dma((team,))] * 2
+        + [dma((4,))] * 2
         + [dma(())] * 2
         + [dma((per,))] * 4
         + [dma((n,))] * 4

time: 72 us -> 82.9 us (1.15)
  the two profiles are of different devices: /device:TPU:1 before, /device:TPU:21 now
where the time goes in v3:
time: 82.9 us; the launch traced here: 82.8 us
  Pallas kernels  82.1 us (99%)
    pallas_call x1, Pallas kernels, fused(): pl.pallas_call(functools.partial(fused_kernel, n, groups), out_shape=(hel...  80.1 us
    pallas_call x1, Pallas kernels, settle(): pl.pallas_call(functools.partial(settle_kernel, count), out_shape=tuple((...  1.97 us

profile of v3, /device:TPU:21, one launch (start us, length us, event | category | flops | bytes accessed | tf_op | source)
XLA Modules:
  0.0 82.8 jit_solution(7027328534864132958)
XLA Ops:
  0.6 80.1 %shard_map.179 = (bf16[2048,256]{1,0:T(8,128)(2,1)S(1)}, bf16[2048,256]{1,0:T(8,128)(2,1)S(1)}, bf16[256,2048]{1,0:T(8,128)(2,1)S(1)}, bf16[192,512]{1,0:T(8,128...) custom-call(bf16[192,2048]{1,0:T(8,128)(2,1)} %out_grad_hbm.1, ...), custom_call_target="tpu_custom_call" | custom-call | tf_op jit(solution)/shard_map/pallas_call | solution.py:1212
  80.8 2.0 %shard_map.180 = (bf16[2048,256]{1,0:T(8,128)(2,1)}, bf16[2048,256]{1,0:T(8,128)(2,1)}, bf16[256,2048]{1,0:T(8,128)(2,1)}, bf16[192,512]{1,0:T(8,128)(2,1)}, f32...) custom-call(bf16[2048,256]{1,0:T(8,128)(2,1)S(1)} %get-tuple-element.24.refs_0_, ...), custom_call_target="tpu_custom_call" | custom-call | tf_op jit(solution)/shard_map/pallas_call | solution.py:1159

commit v4 on v2

--- a/solution.py
+++ b/solution.py
@@ -984,7 +984,6 @@
     out_gate_out[...] = (gated_grad * conv[...]).astype(BF16)
     for q in range(deep):
         gated_over(q).wait_recv()
-    weight_out[...] = dot_tn(wide[:, slice_at(me)], gated[me])
     holder = lax.rem(lax.div(me, per), 2)
 
     def meet(off, carry):
@@ -999,10 +998,13 @@
         def _():
             slice_relay(s).wait_recv()
 
-        weight_out[...] += dot_tn(slices[s], gated[s])
         return carry
 
     lax.fori_loop(1, n, meet, 0)
+    slices[me] = wide[:, slice_at(me)]
+    weight_out[...] = dot_tn(
+        slices[...].reshape(n * tokens, span), gated[...].reshape(n * tokens, gated.shape[2])
+    )
     back_rim.wait_recv()
     follow[pl.ds(tokens, 8)] = jnp.where(me == n - 1, 0.0, later[...])
     mixed_grad = taps[0:1, :] * follow[pl.ds(0, tokens)]

time: 72 us -> 72.1 us (level)
  no operation moved by 1% of the time
where the time goes in v4:
time: 72.1 us; the launch traced here: 71.5 us
  Pallas kernels  70.9 us (98%)
    pallas_call x1, Pallas kernels, fused(): pl.pallas_call(functools.partial(fused_kernel, n, groups), out_shape=(hel...  68.9 us
    pallas_call x1, Pallas kernels, settle(): pl.pallas_call(functools.partial(settle_kernel, count), out_shape=tuple((...  1.97 us

profile of v4, /device:TPU:1, one launch (start us, length us, event | category | flops | bytes accessed | tf_op | source)
XLA Modules:
  0.0 71.5 jit_solution(12451864177766495006)
XLA Ops:
  0.6 68.9 %shard_map.179 = (bf16[2048,256]{1,0:T(8,128)(2,1)S(1)}, bf16[2048,256]{1,0:T(8,128)(2,1)S(1)}, bf16[256,2048]{1,0:T(8,128)(2,1)S(1)}, bf16[192,512]{1,0:T(8,128...) custom-call(bf16[192,2048]{1,0:T(8,128)(2,1)} %out_grad_hbm.1, ...), custom_call_target="tpu_custom_call" | custom-call | tf_op jit(solution)/shard_map/pallas_call | solution.py:1124
  69.5 2.0 %shard_map.180 = (bf16[2048,256]{1,0:T(8,128)(2,1)}, bf16[2048,256]{1,0:T(8,128)(2,1)}, bf16[256,2048]{1,0:T(8,128)(2,1)}, bf16[192,512]{1,0:T(8,128)(2,1)}, f32...) custom-call(bf16[2048,256]{1,0:T(8,128)(2,1)S(1)} %get-tuple-element.24.refs_0_, ...), custom_call_target="tpu_custom_call" | custom-call | tf_op jit(solution)/shard_map/pallas_call | solution.py:1071
